TPU v7x, 512 devices: a whole 4x4x16 slice. The times are simulated.
512 devices in a mesh: sp: 64 (over z, y), tp: 8 (over x, core).
Axes of the slice: x: 4, y: 4, z: 16, core: 2. Of those that a mesh axis runs over, the one named last changes fastest.
Arguments:
- resid: bfloat16 [12288, 2048], P('sp'), may hold values from -6 to 6
- queries: bfloat16 [12288, 1024], P('sp', 'tp'), may hold values from -6.5 to 6.5
- keys: bfloat16 [12288, 1024], P('sp', 'tp'), may hold values from -6.5 to 6.5
- values: bfloat16 [12288, 1024], P('sp', 'tp'), may hold values from -6 to 6
- lambdas: float32 [8], P('tp'), may hold values from 0.3 to 0.8
- head_gain: float32 [128], replicated, may hold values from 0.1 to 1.9
- out_weight: bfloat16 [1024, 2048], P('tp'), may hold values from -0.1875 to 0.1875
- norm_gain: float32 [2048], replicated, may hold values from 0.1 to 1.9
- gate_weight: bfloat16 [2048, 5632], P('sp', 'tp'), may hold values from -0.125 to 0.125
- up_weight: bfloat16 [2048, 5632], P('sp', 'tp'), may hold values from -0.125 to 0.125
- down_weight: bfloat16 [5632, 2048], P('tp', 'sp'), may hold values from -0.078125 to 0.078125
Outputs:
- result: bfloat16 [12288, 2048], P('sp')
All inputs are finite; a program needn't handle non-finite values.
Results may differ from a plain program's by a relative error of at most 0.014.
Values may be sent and summed in bfloat16 or wider, within the bound.
A program may use at most 128 MiB of HBM per device.

v0:
```python
import jax
import jax.numpy as jnp
from jax import lax
from jax.sharding import Mesh
from jax.sharding import PartitionSpec as P

QK = 64
VD = 128
SP = ("sp_0", "sp_1")


def sent_together(arrays, axis, dim, along):
    widths = [a.shape[along] for a in arrays]
    both = jnp.concatenate(arrays, axis=along)
    filled = lax.all_gather(both, axis, axis=dim, tiled=True)
    return tuple(jnp.split(filled, [sum(widths[:k]) for k in range(1, len(widths))], axis=along))


def gathered_by_axis(value, axes, dim):
    if not axes:
        return value
    nearer = lax.all_gather(value, axes[-1], axis=dim, tiled=True)
    return gathered_by_axis(nearer, axes[:-1], dim)


def cut_along(value, dim, devices):
    dims = value.shape
    parts = value.reshape(*dims[:dim], devices, dims[dim] // devices, *dims[dim + 1 :])
    return jnp.moveaxis(parts, dim, 0)


def sent_and_summed(value, axis, dim):
    parts = cut_along(value, dim, lax.axis_size(axis))
    arrived = lax.all_to_all(parts, axis, split_axis=0, concat_axis=0, tiled=True)
    return arrived.astype(jnp.float32).sum(axis=0)


def copy_for_each(value, axis):
    copies = jnp.broadcast_to(value, (lax.axis_size(axis), *value.shape))
    return lax.all_to_all(copies, axis, split_axis=0, concat_axis=0, tiled=True)


def laid_out(parts, dim):
    parts = jnp.moveaxis(parts, 0, dim)
    dims = parts.shape
    return parts.reshape(*dims[:dim], dims[dim] * dims[dim + 1], *dims[dim + 2 :])


def gather_directly(value, axis, dim):
    parts = copy_for_each(value, axis)
    return laid_out(parts, dim)


def rms_rows(first, norm_gain):
    return (
        first * lax.rsqrt(jnp.mean(first * first, axis=-1, keepdims=True) + 1e-06) * norm_gain
    ).astype(jnp.bfloat16)


def local(
    resid,
    queries,
    keys,
    values,
    lambdas,
    head_gain,
    out_weight,
    norm_gain,
    gate_weight,
    up_weight,
    down_weight,
):
    early_pair = sent_together((gate_weight, up_weight), SP, 0, 1)
    early_down = gathered_by_axis(down_weight, SP, 1)
    tok_rows = queries.shape[0]
    local_heads = lambdas.shape[0]
    model_width = resid.shape[1]
    offset = lax.axis_index(SP) * tok_rows
    query_four = queries.reshape(tok_rows, local_heads, 2, QK)
    score_scale = QK ** (-0.5)
    query_pos = offset + lax.iota(jnp.int32, tok_rows)
    last_query = offset + tok_rows - 1

    def update(fold_state, key_part, value_part, key_pos):
        run_max, run_sum, run_acc = fold_state
        scores = (
            jnp.einsum("qhcd,khcd->chqk", query_four, key_part, preferred_element_type=jnp.float32)
            * score_scale
        )
        causal_mask = key_pos[None, :] <= query_pos[:, None]
        scores = jnp.where(causal_mask, scores, -1e30)
        new_max = jnp.maximum(run_max, jnp.max(scores, axis=-1))
        expo = jnp.where(causal_mask, jnp.exp(scores - new_max[..., None]), 0.0)
        factor = jnp.exp(run_max - new_max)
        new_sum = run_sum * factor + jnp.sum(expo, axis=-1)
        new_acc = run_acc * factor[..., None] + jnp.einsum(
            "chqk,khd->chqd",
            expo.astype(jnp.bfloat16),
            value_part,
            preferred_element_type=jnp.float32,
        )
        return (new_max, new_sum, new_acc)

    initial = (
        jnp.full((2, local_heads, tok_rows), -1e30, jnp.float32),
        jnp.zeros((2, local_heads, tok_rows), jnp.float32),
        jnp.zeros((2, local_heads, tok_rows, VD), jnp.float32),
    )
    key_rows, value_rows = sent_together((keys, values), SP, 0, 1)
    key_count = key_rows.shape[0]
    key_span = key_count
    while key_span > 1024 and key_span % 2 == 0:
        key_span = key_span // 2

    def one_span(span_index, inner_state):
        span_start = span_index * key_span
        key_part = lax.dynamic_slice_in_dim(key_rows, span_start, key_span, 0).reshape(
            key_span, local_heads, 2, QK
        )
        value_part = lax.dynamic_slice_in_dim(value_rows, span_start, key_span, 0).reshape(
            key_span, local_heads, VD
        )
        key_pos = span_start + lax.iota(jnp.int32, key_span)
        return update(inner_state, key_part, value_part, key_pos)

    def run_spans(inner_state):
        return lax.fori_loop(0, key_count // key_span, one_span, inner_state)

    def keep_state(inner_state):
        return inner_state

    final_max, final_sum, final_acc = lax.cond(
        jnp.int32(0) <= last_query, run_spans, keep_state, initial
    )
    ratio = final_acc / final_sum[..., None]
    mixed_heads = ratio[0] - lambdas[:, None, None] * ratio[1]
    head_out = (
        mixed_heads
        * lax.rsqrt(jnp.mean(mixed_heads * mixed_heads, axis=-1, keepdims=True) + 1e-05)
        * head_gain
    ).astype(jnp.bfloat16)
    out_three = out_weight.reshape(local_heads, VD, model_width)
    own_count = tok_rows // lax.axis_size("tp")
    branch = sent_and_summed(
        jnp.einsum("hqd,hde->qe", head_out, out_three, preferred_element_type=jnp.float32).astype(
            jnp.bfloat16
        ),
        "tp",
        0,
    )
    resid_own = lax.dynamic_slice_in_dim(resid, lax.axis_index("tp") * own_count, own_count, 0)
    first = resid_own.astype(jnp.float32) + branch
    normed_all = gather_directly(rms_rows(first, norm_gain), "tp", 0)
    gate_act = jnp.dot(normed_all, early_pair[0], preferred_element_type=jnp.float32)
    up_act = jnp.dot(normed_all, early_pair[1], preferred_element_type=jnp.float32)
    hidden = (jax.nn.silu(gate_act) * up_act).astype(jnp.bfloat16)
    terms = jnp.dot(hidden, early_down, preferred_element_type=jnp.float32)
    mixer = sent_and_summed(terms.astype(jnp.bfloat16), "tp", 0)
    finished = (first + 0.5 * mixer).astype(jnp.bfloat16)
    return gather_directly(finished, "tp", 0)


def solution(mesh):
    finer = Mesh(mesh.devices.reshape(16, 4, mesh.shape["tp"]), ("sp_0", "sp_1", "tp"))
    return jax.shard_map(
        local,
        mesh=finer,
        in_specs=(
            P(SP, None),
            P(SP, "tp"),
            P(SP, "tp"),
            P(SP, "tp"),
            P("tp"),
            P(),
            P("tp", None),
            P(),
            P(SP, "tp"),
            P(SP, "tp"),
            P("tp", SP),
        ),
        out_specs=P(SP, None),
        check_vma=False,
    )
```

profile of v0, /device:TPU:1, one launch (start us, length us, event | category | flops | bytes accessed | tf_op | source)
XLA Modules:
  0.0 432.9 jit_solution(256926748074529515)
XLA Ops:
  9.8 12.5 %all_gather.14 = bf16[704,128]{0,1:T(8,128)(2,1)} all-gather(bf16[704,32]{0,1:T(8,128)(2,1)} %param.25), channel_id=1, replica_groups=mesh['sp_0'=16,'sp_1'=4,'tp'=8] {'sp_1'}, dimensions={1}, use_global_device_ids=true | all-gather | bytes 225280 | tf_op jit(solution)/shard_map/all_gather | solution.py:22
  22.9 135.4 %all-gather.4.cloned.1.call-done = bf16[12288,256]{1,0:T(8,128)(2,1)} async-done(((bf16[192,256]{1,0:T(8,128)(2,1)}), bf16[12288,256]{1,0:T(8,128)(2,1)}) %all-gather.4.cloned.1.call-update) | async-done | bytes 6291472 | tf_op jit(solution)/shard_map/all_gather | solution.py:15
  158.3 102.5 %conditional.1 = (f32[2,1,192]{2,0,1:T(2,128)}, f32[2,1,192,128]{3,2,0,1:T(8,128)}) conditional(s32[]{:T(128)} %convert_element_type.43, () %tuple.27, (bf16[12288,256]{1,0:T(8,128)(2,1)}, bf16[192,128]{1,0:T(8,128)(2,1)}, s32[]{:T(128)}, s32[192]{0:T(256)S(1)}) %tuple.28), branch_computations={%region_0.0_spmd, %region_1.6_spmd} | conditional | flops 116198600 | bytes 56017520 | solution.py:132
  158.3 8.6 %copy.13 = bf16[12288,256]{0,1:T(8,128)(2,1)} copy(bf16[12288,256]{1,0:T(8,128)(2,1)} %get-tuple-element.159) | data formatting | bytes 12582912 | tf_op jit(solution)/shard_map
  166.9 4.0 split.16
  173.6 87.1 %while.17 = (s32[]{:T(128)}, f32[2,1,192]{2,0,1:T(2,128)S(1)}, f32[2,1,192]{2,0,1:T(2,128)}, f32[2,1,192,128]{3,2,0,1:T(8,128)}, s32[192]{0:T(256)S(1)}, /*index...) while((s32[]{:T(128)}, f32[2,1,192]{2,0,1:T(2,128)S(1)}, ...), condition=%wide.region_5.5_spmd.clone, body=%wide.region_2.4_spmd.clone.sunk | while | flops 116198408 | bytes 5389243 | solution.py:127
  175.3 2.1 fusion.60
  180.0 2.1 fusion.60
  185.5 2.1 fusion.60
  191.0 2.1 fusion.60
  196.5 2.1 fusion.60
  202.0 2.1 fusion.60
  207.5 2.1 fusion.60
  213.0 2.1 fusion.60
  218.5 2.1 fusion.60
  223.9 2.1 fusion.60
  229.4 2.1 fusion.60
  234.9 2.1 fusion.60
  240.4 2.1 fusion.60
  245.9 2.1 fusion.60
  251.4 2.1 fusion.60
  256.9 2.1 fusion.60
  263.3 13.1 %all-to-all-start = ((bf16[8,24,2048]{2,1,0:T(8,128)(2,1)}), bf16[8,24,2048]{2,1,0:T(8,128)(2,1)S(1)}, u32[]{:S(2)}, u32[]{:S(2)}) async-start(bf16[8,24,2048]{2,1,0:T(8,128)(2,1)} %bitcast.4), calls=%async_computation | async-start | bytes 1572864 | tf_op jit(solution)/shard_map/all_to_all | solution.py:34
  276.4 12.2 %all-to-all-done = bf16[8,24,2048]{2,1,0:T(8,128)(2,1)S(1)} async-done(((bf16[8,24,2048]{2,1,0:T(8,128)(2,1)}), bf16[8,24,2048]{2,1,0:T(8,128)(2,1)S(1)}, u32[]{:S(2)}, u32[]{:S(2)}) %all-to-all-start) | async-done | bytes 786464 | tf_op jit(solution)/shard_map/all_to_all | solution.py:34
  291.7 4.4 %all-to-all-start.1 = ((bf16[8,24,2048]{2,1,0:T(8,128)(2,1)}), bf16[8,24,2048]{2,1,0:T(8,128)(2,1)S(1)}, u32[]{:S(2)}, u32[]{:S(2)}) async-start(bf16[8,24,2048]{2,1,0:T(8,128)(2,1)} %broadcast_in_dim.57), calls=%async_computation.1 | async-start | bytes 1572864 | tf_op jit(solution)/shard_map/all_to_all | solution.py:40
  296.1 9.9 %all-gather.6.cloned.1.call-done = bf16[2048,1408]{1,0:T(8,128)(2,1)} async-done(((bf16[32,1408]{1,0:T(8,128)(2,1)}), bf16[2048,1408]{1,0:T(8,128)(2,1)}) %all-gather.6.cloned.1.call-update) | async-done | bytes 5767184 | tf_op jit(solution)/shard_map/all_gather | solution.py:15
  306.0 2.3 all-to-all-done.1
  308.3 2.7 fusion.17
  311.0 67.0 %all-gather.8.cloned.1.call-done = bf16[704,2048]{0,1:T(8,128)(2,1)} async-done(((bf16[704,128]{0,1:T(8,128)(2,1)}), bf16[704,2048]{0,1:T(8,128)(2,1)}) %all-gather.8.cloned.1.call-update) | async-done | bytes 2883600 | tf_op jit(solution)/shard_map/all_gather | solution.py:22
  378.0 5.0 %convolution_convert_fusion = bf16[192,2048]{1,0:T(8,128)(2,1)S(1)} fusion(bf16[704,2048]{0,1:T(8,128)(2,1)} %all-gather.8.cloned.1.call-done, bf16[192,2048]{1,0:T(8,128)(2,1)S(1)} %bitcast.70, bf16[2048,1408]{1,0:T(8,128)(2,1)} %all-gather.6.cloned.1.call-done, f32[192,704]{1,0:T(8,128)S(1)} %fusion.17), kind=kOutput, calls=%fused_computation.31 | convolution fusion | flops 1108500480 | bytes 8404992 | tf_op jit(solution)/shard_map/dot_general | solution.py:157
  383.0 25.8 %all_to_all.20 = bf16[8,24,2048]{2,1,0:T(8,128)(2,1)S(1)} all-to-all(bf16[8,24,2048]{2,1,0:T(8,128)(2,1)S(1)} %bitcast.71), channel_id=1, replica_groups=mesh['sp_0'=16,'sp_1'=4,'tp'=8] {'tp'}, dimensions={0} | all-to-all | bytes 1572864 | tf_op jit(solution)/shard_map/all_to_all | solution.py:34
  409.9 15.6 %all_to_all.21 = bf16[8,24,2048]{2,1,0:T(8,128)(2,1)S(1)} all-to-all(bf16[8,24,2048]{2,1,0:T(8,128)(2,1)S(1)} %broadcast_in_dim.58), channel_id=1, replica_groups=mesh['sp_0'=16,'sp_1'=4,'tp'=8] {'tp'}, dimensions={0} | all-to-all | bytes 1572864 | tf_op jit(solution)/shard_map/all_to_all | solution.py:40
  (166 shorter events, 66.0 us)
Async XLA Ops:
  6.5 255.4 %copy-start = (bf16[128,2048]{1,0:T(8,128)(2,1)S(1)}, bf16[128,2048]{1,0:T(8,128)(2,1)}, u32[]{:S(2)}) copy-start(bf16[128,2048]{1,0:T(8,128)(2,1)} %param.21) | copy-start | bytes 1572868
  6.5 151.8 %all-gather.4.cloned.1.call-start = ((), (), s32[]{:S(2)}) async-start(), calls=%async_computation.4 | async-start | bytes 6389760 | tf_op jit(solution)/shard_map/all_gather | solution.py:15
  8.1 297.9 %all-gather.6.cloned.1.call-start = ((), (), s32[]{:S(2)}) async-start(), calls=%async_computation.5 | async-start | bytes 5857280 | tf_op jit(solution)/shard_map/all_gather | solution.py:15
  9.7 368.3 %all-gather.8.cloned.1.call-start = ((), (), s32[]{:S(2)}) async-start(), calls=%async_computation.6 | async-start | bytes 3342336 | tf_op jit(solution)/shard_map/all_gather | solution.py:22
  158.3 103.7 %copy-start.4 = (f32[128]{0:T(128)S(1)}, f32[128]{0:T(128)}, u32[]{:S(2)}) copy-start(f32[128]{0:T(128)} %param.20) | copy-start | bytes 1540
  166.9 4.8 %copy-start.1 = (bf16[12288,256]{1,0:T(8,128)(2,1)S(1)}, bf16[12288,256]{1,0:T(8,128)(2,1)}, u32[]{:S(2)}) copy-start(bf16[12288,256]{1,0:T(8,128)(2,1)} %get-tuple-element.159) | copy-start | bytes 18874372 | tf_op jit(solution)/shard_map/cond
  171.7 1.8 copy-start.2
  263.3 26.5 %copy-start.3 = (f32[2048]{0:T(1024)S(1)}, f32[2048]{0:T(1024)}, u32[]{:S(2)}) copy-start(f32[2048]{0:T(1024)} %param.22) | copy-start | bytes 24580
  263.3 25.3 %all-to-all-start = ((bf16[8,24,2048]{2,1,0:T(8,128)(2,1)}), bf16[8,24,2048]{2,1,0:T(8,128)(2,1)S(1)}, u32[]{:S(2)}, u32[]{:S(2)}) async-start(bf16[8,24,2048]{2,1,0:T(8,128)(2,1)} %bitcast.4), calls=%async_computation | async-start | bytes 1572864 | tf_op jit(solution)/shard_map/all_to_all | solution.py:34
  291.7 16.6 %all-to-all-start.1 = ((bf16[8,24,2048]{2,1,0:T(8,128)(2,1)}), bf16[8,24,2048]{2,1,0:T(8,128)(2,1)S(1)}, u32[]{:S(2)}, u32[]{:S(2)}) async-start(bf16[8,24,2048]{2,1,0:T(8,128)(2,1)} %broadcast_in_dim.57), calls=%async_computation.1 | async-start | bytes 1572864 | tf_op jit(solution)/shard_map/all_to_all | solution.py:40
Sparse Core Ops, SparseCore 0:
  10.3 147.9 all-gather.3
  161.2 144.7 all-gather.5
  308.1 69.8 all-gather.7
where the time goes:
time: 435 us; the launch traced here: 433 us
  waiting for transfers between devices  227 us (52%)
  blocking collectives  53.8 us (12%)
  matrix products  51.3 us (12%)
  other arithmetic  36.8 us (8%)
  local copies, waits for them, and re-layouts  32.3 us (7%)
  starting transfers between devices  17.7 us (4%)
  between operations  13.8 us (3%)
    all_gather x2, waiting for transfers between devices, sent_together(): filled = lax.all_gather(both, axis, axis=dim, tiled=True)  145 us
    all_gather x1, waiting for transfers between devices, gathered_by_axis(): nearer = lax.all_gather(value, axes[-1], axis=dim, tiled=True)  67 us
    dot_general x16, matrix products, update(): jnp.einsum('chqk,khd->chqd', expo.astype(jnp.bfloat16), value_part, prefe...  34.2 us
    all_to_all x1, blocking collectives, sent_and_summed(): lax.all_to_all(parts, axis, split_axis=0, concat_axis=0, tiled=True)  25.8 us
    add x16, other arithmetic, update(): new_sum = run_sum * factor + jnp.sum(expo, axis=-1)  19.9 us
    all_to_all x1, blocking collectives, copy_for_each(): return lax.all_to_all(copies, axis, split_axis=0, concat_axis=0, tiled=True)  15.6 us
    dynamic_slice x16, local copies, waits for them, and re-layouts, one_span(): lax.dynamic_slice_in_dim(key_rows, span_start, key_span, 0)  15 us
    all_to_all x1, starting transfers between devices, sent_and_summed(): lax.all_to_all(parts, axis, split_axis=0, concat_axis=0, tiled=True)  13.1 us
  transfers between devices with their start and end apart: 5, of which 5 were waited for; matrix products, arithmetic and copies ran while one was open for 26% of the time, Pallas kernels for 0%

commit v1 on v0

v1 whole, which is shorter than its diff:
```python
import functools
import math

import jax
import jax.numpy as jnp
from jax import lax
from jax.experimental import pallas as pl
from jax.experimental.pallas import tpu as pltpu
from jax.sharding import Mesh
from jax.sharding import PartitionSpec as P

QK = 64
VD = 128
LANES = 128
NC = 2
SP = ("z", "y")
TP = ("x", "c")
MESH = pl.DeviceIdType.MESH
SEMS = 200
SCALE2 = QK ** (-0.5) * math.log2(math.e)
NEG = -1e30


def dot_nt(a, b):
    return lax.dot_general(a, b, (((1,), (1,)), ((), ())), preferred_element_type=jnp.float32)


def dot_nn(a, b):
    return jnp.dot(a, b, preferred_element_type=jnp.float32)


def kernel(
    nz,
    ny,
    nx,
    lam_ref,
    q_ref,
    k_ref,
    v_ref,
    hg_ref,
    ow_ref,
    ng_ref,
    resid_ref,
    gu_ref,
    dn_ref,
    out_ref,
    kb,
    vb,
    qb,
    qm,
    acc,
    mx,
    ls,
    rb,
    mb,
    gu,
    dstage,
    dn,
    pf,
    pown,
    pair,
    sx,
    rx,
    first,
    ss,
    ss_in,
    nall,
    fb,
    fown,
    pair2,
    gs,
    ra,
    rbx,
    sa,
    sb,
    ra2,
    rb2,
    send_sem,
    recv_sem,
):
    z, y, x, c = (lax.axis_index(a) for a in ("z", "y", "x", "c"))
    R = q_ref.shape[0]
    Rx = R // nx
    Dc = resid_ref.shape[1] // NC
    D = NC * Dc
    H = Dc // 2
    h = dn_ref.shape[1]
    GR = ny * gu_ref.shape[1]
    RS = gu_ref.shape[1]
    bf = jnp.bfloat16
    f32 = jnp.float32

    def at(axis, d):
        me, n = {"z": (z, nz), "y": (y, ny), "x": (x, nx)}[axis]
        return lax.rem(me + (d + n), n)

    def mult(v, m):
        return pl.multiple_of(v, m)

    up, down = {"z": at("z", 1)}, {"z": at("z", -1)}
    partner = {"c": 1 - c}
    peers = [up, down, partner]
    peers += [{"y": at("y", d)} for d in range(1, ny)]
    peers += [{"x": at("x", d)} for d in range(1, nx)]
    barrier = pltpu.get_barrier_semaphore()
    for p in peers:
        pl.semaphore_signal(barrier, inc=1, device_id=p, device_id_type=MESH)
    pl.semaphore_wait(barrier, len(peers))

    started = []

    def send(src, dst, to):
        k = len(started)
        copy = pltpu.make_async_remote_copy(
            src_ref=src,
            dst_ref=dst,
            send_sem=send_sem.at[k],
            recv_sem=recv_sem.at[k],
            device_id=to,
            device_id_type=MESH,
        )
        copy.start()
        started.append(copy)
        return copy

    U, W = nz // 2, (nz - 1) // 2
    ku, vu, kd, vd = ({} for _ in range(4))
    ku[1] = send(k_ref, kb.at[z], up)
    kd[1] = send(k_ref, kb.at[z], down)
    qs = [send(q_ref, qb.at[y], {"y": at("y", d)}) for d in range(1, ny)]
    vu[1] = send(v_ref, vb.at[z], up)
    vd[1] = send(v_ref, vb.at[z], down)

    def gu_slot(zz):
        return gu.at[pl.ds(mult(zz * GR, GR), GR)]

    def dn_slot(zz):
        return dn.at[pl.ds(0, h), pl.ds(mult(zz * LANES, LANES), LANES)]

    ws = []
    for d in range(1, ny):
        to = at("y", d)
        row = mult(z * GR + y * RS, RS)
        ws.append(send(gu_ref.at[to], gu.at[pl.ds(row, RS)], {"y": to}))
        ws.append(send(dn_ref.at[to], dstage.at[y], {"y": to}))

    qb[y] = q_ref[...]
    gu[pl.ds(mult(z * GR + y * RS, RS), RS), :] = gu_ref[y]
    dn[pl.ds(h, dn.shape[0] - h), :] = jnp.zeros((dn.shape[0] - h, D), bf)
    for a in qs:
        a.wait_recv()
    lane = lax.broadcasted_iota(jnp.int32, (R, LANES), 1)
    for yy in range(ny):
        block = qb[yy]
        zero = jnp.zeros_like(block)
        qm[yy * R : (yy + 1) * R, :] = jnp.where(lane < QK, block, zero)
        qm[(ny + yy) * R : (ny + yy + 1) * R, :] = jnp.where(lane < QK, zero, block)
    acc[...] = jnp.zeros_like(acc)
    ls[...] = jnp.zeros_like(ls)
    mx[...] = jnp.full(mx.shape, NEG, f32)

    def attend(load, masked):
        def body(i, carry):
            rows = pl.ds(mult(i * R, R), R)
            keys, vals = load()
            s = dot_nt(qm[rows, :], keys)
            if masked:
                kpos = y * R + lax.broadcasted_iota(jnp.int32, s.shape, 1)
                qpos = lax.rem(i, ny) * R + lax.broadcasted_iota(jnp.int32, s.shape, 0)
                keep = kpos <= qpos
                s = jnp.where(keep, s, NEG)
            old = mx[rows, :]
            new = jnp.maximum(old, jnp.max(s, axis=-1, keepdims=True))
            e = jnp.exp2((s - new[:, :1]) * SCALE2)
            if masked:
                e = jnp.where(keep, e, 0.0)
            factor = jnp.exp2((old - new) * SCALE2)
            mx[rows, :] = new
            ls[rows, :] = ls[rows, :] * factor + jnp.sum(e, axis=-1, keepdims=True)
            acc[rows, :] = acc[rows, :] * factor + dot_nn(e.astype(bf), vals)
            return carry

        lax.fori_loop(0, 2 * ny, body, 0)

    attend(lambda: (k_ref[...], v_ref[...]), True)

    for a in ws:
        a.wait_recv()
    dn_mine = dn_ref[y]
    for d in range(1, ny):
        dn_mine = dn_mine + dstage[at("y", -d)]
    dn[pl.ds(0, h), pl.ds(mult(z * LANES, LANES), LANES)] = dn_mine

    for s in range(1, U + 1):
        zu, zd = at("z", -s), at("z", s)
        ku[s].wait_recv()
        if s < U:
            ku[s + 1] = send(kb.at[zu], kb.at[zu], up)
        if s <= W:
            kd[s].wait_recv()
            if s < W:
                kd[s + 1] = send(kb.at[zd], kb.at[zd], down)
        vu[s].wait_recv()
        if s < U:
            vu[s + 1] = send(vb.at[zu], vb.at[zu], up)
        if s <= W:
            vd[s].wait_recv()
            if s < W:
                vd[s + 1] = send(vb.at[zd], vb.at[zd], down)

        def one(zu=zu):
            attend(lambda: (kb[zu], vb[zu]), False)

        def two(zu=zu, zd=zd):
            attend(
                lambda: (
                    jnp.concatenate([kb[zu], kb[zd]], axis=0),
                    jnp.concatenate([vb[zu], vb[zd]], axis=0),
                ),
                False,
            )

        if s <= W:
            pl.when(z >= nz - s)(two)
            pl.when((z >= s) & (z < nz - s))(one)
        else:
            pl.when(z >= s)(one)

    gu_u, dn_u, gu_d, dn_d = ({} for _ in range(4))

    def weight_step(s):
        if s > U:
            return
        zu, zd = at("z", -s), at("z", s)
        if s > 0:
            gu_u[s].wait_recv()
        if s < U:
            gu_u[s + 1] = send(gu_slot(zu), gu_slot(zu), up)
        if 0 < s <= W:
            gu_d[s].wait_recv()
        if s < W:
            gu_d[s + 1] = send(gu_slot(zd), gu_slot(zd), down)
        if s > 0:
            dn_u[s].wait_recv()
        if s < U:
            dn_u[s + 1] = send(dn_slot(zu), dn_slot(zu), up)
        if 0 < s <= W:
            dn_d[s].wait_recv()
        if s < W:
            dn_d[s + 1] = send(dn_slot(zd), dn_slot(zd), down)

    weight_step(0)

    def partial(yy):
        tile = jnp.zeros((R, LANES), f32)
        for m in range(2):
            rows = pl.ds(mult((m * ny + yy) * R, R), R)
            total = ls[rows, :]
            some = total > 0.0
            safe = jnp.where(some, total, 1.0)
            rb[yy, :, m * VD : (m + 1) * VD] = (acc[rows, :] / safe).astype(bf)
            lse = jnp.where(some, mx[rows, :] * SCALE2 + jnp.log2(safe), NEG)
            high = lse.astype(bf).astype(f32)
            rest = lse - high
            middle = rest.astype(bf).astype(f32)
            low = rest - middle
            for j, piece in enumerate((high, middle, low)):
                tile = jnp.where(lane == 3 * m + j, piece, tile)
        rb[yy, :, 2 * VD :] = tile.astype(bf)

    ms = []
    for d in range(1, ny):
        to = at("y", d)
        partial(to)
        ms.append(send(rb.at[to], mb.at[y], {"y": to}))
    partial(y)
    weight_step(1)
    for a in ms:
        a.wait_recv()
    parts = [rb.at[y]] + [mb.at[at("y", -d)] for d in range(1, ny)]
    ratios = []
    for m in range(2):
        lses = []
        for part in parts:
            t = part[:, 2 * VD :].astype(f32)
            mine = (lane >= 3 * m) & (lane < 3 * m + 3)
            lses.append(jnp.sum(jnp.where(mine, t, 0.0), axis=-1, keepdims=True))
        top = functools.reduce(jnp.maximum, lses)
        weights = [jnp.exp2(v - top) for v in lses]
        total = functools.reduce(jnp.add, weights)
        numer = functools.reduce(
            jnp.add,
            [w * part[:, m * VD : (m + 1) * VD].astype(f32) for w, part in zip(weights, parts)],
        )
        ratios.append(numer / total)
    mixed = ratios[0] - lam_ref[0] * ratios[1]
    head = (
        mixed
        * lax.rsqrt(jnp.mean(mixed * mixed, axis=-1, keepdims=True) + 1e-05)
        * hg_ref[...]
    ).astype(bf)

    other_cols = pl.ds(mult((1 - c) * Dc, Dc), Dc)
    own_cols = pl.ds(mult(c * Dc, Dc), Dc)
    pf[...] = dot_nn(head, ow_ref[:, other_cols]).astype(bf)
    pc = send(pf, pair, partner)
    pown[...] = dot_nn(head, ow_ref[:, own_cols])
    weight_step(2)
    pc.wait_recv()
    xs = []
    for d in range(1, nx):
        to = at("x", d)
        rows = pl.ds(mult(to * Rx, Rx), Rx)
        sx[rows, :] = (pown[rows, :] + pair[rows, :].astype(f32)).astype(bf)
        xs.append(send(sx.at[rows], rx.at[x], {"x": to}))
    my_rows = pl.ds(mult(x * Rx, Rx), Rx)
    total = pown[my_rows, :] + pair[my_rows, :].astype(f32)
    total = total + resid_ref[my_rows, own_cols].astype(f32)
    for a in xs:
        a.wait_recv()
    for d in range(1, nx):
        total = total + rx[at("x", -d)].astype(f32)
    first[...] = total
    ss[...] = jnp.broadcast_to(jnp.sum(total * total, axis=-1, keepdims=True), ss.shape)
    sc = send(ss, ss_in, partner)
    weight_step(3)
    sc.wait_recv()
    mean = (ss[...] + ss_in[...])[:, :1] * (1.0 / D)
    normed = (first[...] * lax.rsqrt(mean + 1e-06) * ng_ref[c]).astype(bf)

    def block(yy, xx, half):
        row = mult(yy * R + xx * Rx, Rx)
        return nall.at[c, pl.ds(row, Rx), pl.ds(half * H, H)]

    nall[c, pl.ds(mult(y * R + x * Rx, Rx), Rx), :] = normed

    xa, yb, far_a, far_b, local = {}, {}, [], [], []
    ring = {"x": nx, "y": ny}

    def pass_on(ref, axis):
        return [send(ref, ref, {axis: at(axis, d)}) for d in range(1, ring[axis])]

    first_a = pass_on(block(y, x, 0), "x")
    first_b = pass_on(block(y, x, 1), "y")
    for half, axis, far in ((0, "y", far_a), (1, "x", far_b)):
        far.append(pass_on(block(y, x, half), axis))
        local.append(send(block(y, x, half), block(y, x, half), partner))
    weight_step(4)
    for e in range(1, max(nx, ny)):
        if e < nx:
            first_a[e - 1].wait_recv()
            ref = block(y, at("x", -e), 0)
            far_a.append(pass_on(ref, "y"))
            local.append(send(ref, ref, partner))
        if e < ny:
            first_b[e - 1].wait_recv()
            ref = block(at("y", -e), x, 1)
            far_b.append(pass_on(ref, "x"))
            local.append(send(ref, ref, partner))
    weight_step(5)
    for e in range(max(nx, ny)):
        if e < nx:
            for d in range(1, ny):
                far_a[e][d - 1].wait_recv()
                ref = block(at("y", -d), at("x", -e), 0)
                local.append(send(ref, ref, partner))
        if e < ny:
            for d in range(1, nx):
                far_b[e][d - 1].wait_recv()
                ref = block(at("y", -e), at("x", -d), 1)
                local.append(send(ref, ref, partner))
    for s in range(6, U + 1):
        weight_step(s)
    for a in local:
        a.wait_recv()

    chunk_lane = lax.broadcasted_iota(jnp.int32, (R, LANES), 1)
    p2 = []
    order = [at("y", d) for d in range(1, ny)] + [y]
    for yy in order:
        rows = pl.ds(mult(yy * R, R), R)
        t = dot_nn(nall[0, rows, :], gu[:Dc, :]) + dot_nn(nall[1, rows, :], gu[Dc:, :])
        t0, t1, t2 = (t[:, j * LANES : (j + 1) * LANES] for j in range(3))
        h0 = t0 / (1.0 + jnp.exp(-t0)) * t2
        h1 = t1 / (1.0 + jnp.exp(-t1)) * pltpu.roll(t1, 64, 1)
        h1 = jnp.where(chunk_lane < h - LANES, h1, 0.0)
        hidden = jnp.concatenate([h0, h1], axis=1).astype(bf)
        fb[rows, :] = dot_nn(hidden, dn[:, other_cols]).astype(bf)
        p2.append(send(fb.at[rows], pair2.at[rows], partner))
        fown[rows, :] = dot_nn(hidden, dn[:, own_cols])

    sa1, sb1 = [], []
    left, right = slice(0, H), slice(H, Dc)
    for j, yy in enumerate(order):
        rows = pl.ds(mult(yy * R, R), R)
        p2[j].wait_recv()
        both = fown[rows, :] + pair2[rows, :].astype(f32)
        fown[rows, :] = both
        gs[rows, :] = both.astype(bf)
        if j < ny - 1:
            sa1.append(send(gs.at[rows, left], ra.at[y], {"y": yy}))
        for d in range(1, nx):
            to = at("x", d)
            piece = pl.ds(mult(yy * R + to * Rx, Rx), Rx)
            sb1.append(send(gs.at[piece, right], rbx.at[x, yy], {"x": to}))
    for a in sa1:
        a.wait_recv()
    rows = pl.ds(mult(y * R, R), R)
    half_a = fown[rows, left]
    for d in range(1, ny):
        half_a = half_a + ra[at("y", -d)].astype(f32)
    fown[rows, left] = half_a
    sa[...] = half_a.astype(bf)
    sa2 = []
    for d in range(1, nx):
        to = at("x", d)
        sa2.append(send(sa.at[pl.ds(mult(to * Rx, Rx), Rx)], ra2.at[x], {"x": to}))
    for a in sb1:
        a.wait_recv()
    sb2 = []
    for yy in order:
        piece = pl.ds(mult(yy * R + x * Rx, Rx), Rx)
        half_b = fown[piece, right]
        for d in range(1, nx):
            half_b = half_b + rbx[at("x", -d), yy].astype(f32)
        if len(sb2) < ny - 1:
            sb[yy] = half_b.astype(bf)
            sb2.append(send(sb.at[yy], rb2.at[y], {"y": yy}))
    mine = pl.ds(mult(y * R + x * Rx, Rx), Rx)
    mix_a = fown[mine, left]
    for a in sa2:
        a.wait_recv()
    for d in range(1, nx):
        mix_a = mix_a + ra2[at("x", -d)].astype(f32)
    for a in sb2:
        a.wait_recv()
    mix_b = half_b
    for d in range(1, ny):
        mix_b = mix_b + rb2[at("y", -d)].astype(f32)
    mixer = jnp.concatenate([mix_a, mix_b], axis=1)
    out_ref[my_rows, own_cols] = (first[...] + 0.5 * mixer).astype(bf)

    def tile(xx):
        return out_ref.at[pl.ds(mult(xx * Rx, Rx), Rx), own_cols]

    fx = pass_on(tile(x), "x")
    last = [send(tile(x), tile(x), partner)]
    for d in range(1, nx):
        fx[d - 1].wait_recv()
        ref = tile(at("x", -d))
        last.append(send(ref, ref, partner))
    for a in last:
        a.wait_recv()
    for a in started:
        a.wait_send()


def local(
    nz,
    ny,
    nx,
    resid,
    queries,
    keys,
    values,
    lambdas,
    head_gain,
    out_weight,
    norm_gain,
    gate_weight,
    up_weight,
    down_weight,
):
    R, D = resid.shape
    RS, F = gate_weight.shape
    h = F // ny
    CS = down_weight.shape[1]
    Rx, Dc = R // nx, D // NC
    H = Dc // 2
    bf, f32 = jnp.bfloat16, jnp.float32
    assert LANES < h <= LANES + 64 and CS * ny == LANES and queries.shape[1] == LANES

    def cut(w):
        return jnp.moveaxis(w.reshape(RS, ny, h), 1, 0)

    g, u = cut(gate_weight), cut(up_weight)
    fill = jnp.zeros((ny, RS, 64 - (h - LANES)), bf)
    gu = jnp.concatenate(
        [g[..., :LANES], g[..., LANES:], fill, u[..., LANES:], fill, u[..., :LANES]], axis=-1
    )
    place = lax.broadcasted_iota(jnp.int32, (1, 1, LANES), 2) // CS == lax.axis_index("y")
    dn = jnp.where(place, jnp.tile(down_weight.reshape(ny, h, CS), (1, 1, ny)), 0)

    vm = pl.BlockSpec(memory_space=pltpu.VMEM)
    scratch = [
        ((nz, R, LANES), bf),
        ((nz, R, LANES), bf),
        ((ny, R, LANES), bf),
        ((2 * ny * R, LANES), bf),
        ((2 * ny * R, LANES), f32),
        ((2 * ny * R, LANES), f32),
        ((2 * ny * R, LANES), f32),
        ((ny, R, 3 * LANES), bf),
        ((ny, R, 3 * LANES), bf),
        ((D, 3 * LANES), bf),
        ((ny, h, LANES), bf),
        ((2 * LANES, D), bf),
        ((R, Dc), bf),
        ((R, Dc), f32),
        ((R, Dc), bf),
        ((R, Dc), bf),
        ((nx, Rx, Dc), bf),
        ((Rx, Dc), f32),
        ((Rx, LANES), f32),
        ((Rx, LANES), f32),
        ((NC, ny * R, Dc), bf),
        ((ny * R, Dc), bf),
        ((ny * R, Dc), f32),
        ((ny * R, Dc), bf),
        ((ny * R, Dc), bf),
        ((ny, R, H), bf),
        ((nx, ny, Rx, H), bf),
        ((R, H), bf),
        ((ny, Rx, H), bf),
        ((nx, Rx, H), bf),
        ((ny, Rx, H), bf),
    ]
    return pl.pallas_call(
        functools.partial(kernel, nz, ny, nx),
        out_shape=jax.ShapeDtypeStruct((R, D), bf),
        in_specs=[pl.BlockSpec(memory_space=pltpu.SMEM)] + [vm] * 9,
        out_specs=vm,
        scratch_shapes=[pltpu.VMEM(*s) for s in scratch]
        + [pltpu.SemaphoreType.DMA((SEMS,)), pltpu.SemaphoreType.DMA((SEMS,))],
        compiler_params=pltpu.CompilerParams(
            collective_id=0, has_side_effects=True, vmem_limit_bytes=56 * 1024 * 1024
        ),
    )(
        lambdas,
        queries,
        keys,
        values,
        head_gain.reshape(1, VD),
        out_weight,
        norm_gain.reshape(NC, 1, Dc),
        resid,
        gu,
        dn,
    )


def solution(mesh):
    tp = mesh.shape["tp"]
    sp = mesh.shape["sp"]
    ny = 4 if sp == 64 else 2
    nz, nx = sp // ny, tp // NC
    finer = Mesh(mesh.devices.reshape(nz, ny, nx, NC), ("z", "y", "x", "c"))
    return jax.shard_map(
        functools.partial(local, nz, ny, nx),
        mesh=finer,
        in_specs=(
            P(SP, None),
            P(SP, TP),
            P(SP, TP),
            P(SP, TP),
            P(TP),
            P(),
            P(TP, None),
            P(),
            P(SP, TP),
            P(SP, TP),
            P(TP, SP),
        ),
        out_specs=P(SP, None),
        check_vma=False,
    )
```

time: 435 us -> 137 us (0.31)
  waiting for transfers between devices: 227 us -> 0 us
  Pallas kernels: 0 us -> 130 us
  blocking collectives: 53.8 us -> 0 us
  matrix products: 51.3 us -> 0 us
  other arithmetic: 36.8 us -> 0.7 us
  local copies, waits for them, and re-layouts: 32.3 us -> 5 us
  starting transfers between devices: 17.7 us -> 0 us
  between operations: 13.8 us -> 0.76 us
    all_gather x3 -> x0, waiting for transfers between devices: 212 us -> none  [the longest x2 145 us: sent_together(): filled = lax.all_gather(both, axis, axis=dim, tiled=True)]
    pallas_call x0 -> x1, Pallas kernels: none -> 130 us  [local(): pl.pallas_call(functools.partial(kernel, nz, ny, nx), out_shape=jax.Shape...]
    dot_general x35 -> x0, matrix products: 51.3 us -> none  [the longest x16 34.2 us: update(): jnp.einsum('chqk,khd->chqd', expo.astype(jnp.bfloat16), value_part, prefe...]
    all_to_all x2 -> x0, blocking collectives: 41.3 us -> none  [the longest x1 25.8 us: sent_and_summed(): lax.all_to_all(parts, axis, split_axis=0, concat_axis=0, tiled=True)]
    add x33 -> x0, other arithmetic: 20 us -> none  [the longest x16 19.9 us: update(): new_sum = run_sum * factor + jnp.sum(expo, axis=-1)]
    all_to_all x2 -> x0, starting transfers between devices: 17.6 us -> none  [the longest x1 13.1 us: sent_and_summed(): lax.all_to_all(parts, axis, split_axis=0, concat_axis=0, tiled=True)]
    dynamic_slice x16 -> x0, local copies, waits for them, and re-layouts: 15 us -> none  [one_span(): lax.dynamic_slice_in_dim(key_rows, span_start, key_span, 0)]
    all_to_all x2 -> x0, waiting for transfers between devices: 14.4 us -> none  [the longest x1 12.2 us: sent_and_summed(): lax.all_to_all(parts, axis, split_axis=0, concat_axis=0, tiled=True)]
  transfers between devices with their start and end apart: 5 -> 0, of which waited for: 5 -> 0; matrix products, arithmetic and copies ran while one was open for 26% -> 0% of each run, Pallas kernels for 0% -> 0%
where the time goes in v1:
time: 137 us; the launch traced here: 136 us
  Pallas kernels  130 us (95%)
  local copies, waits for them, and re-layouts  5 us (4%)
    pallas_call x1, Pallas kernels, local(): pl.pallas_call(functools.partial(kernel, nz, ny, nx), out_shape=jax.Shape...  130 us
    unnamed x5, local copies, waits for them, and re-layouts  2.9 us

profile of v1, /device:TPU:1, one launch (start us, length us, event | category | flops | bytes accessed | tf_op | source)
XLA Modules:
  0.0 136.5 jit_solution(5848683334781041351)
XLA Ops:
  0.7 0.9 reshape.57
  1.6 0.0 copy-start
  1.6 0.8 copy-done
  2.4 0.1 reshape.58
  2.6 0.0 copy-start.1
  2.6 0.8 concatenate.3.gu_ref
  3.3 0.0 copy-done.1
  3.4 0.1 tile.10
  3.5 0.2 copy.16
  3.7 0.7 broadcast_select_fusion.dn_ref
  4.4 130.0 %shard_map.109 = bf16[192,2048]{1,0:T(8,128)(2,1)} custom-call(f32[1]{0:T(128)S(6)} %copy.22.lam_ref, bf16[192,128]{1,0:T(8,128)(2,1)} %q_ref.1, bf16[192,128]{1,0:T(8,128)(2,1)} %k_ref.1, bf16[192,128]{1,0:T(8,128)(2,1)} %v_ref.1, f32[1,128]{1,0:T(1,128)} %bitcast.16, bf16[128,2048]{1,0:T(8,128)(2,1)} %ow_ref.1, f32[2,1,1024]{2,1,0:T(1,128)} %bitcast.15, ...), custom_call_target="tpu_custom_call" | custom-call | tf_op jit(solution)/shard_map/pallas_call | solution.py:528
  134.4 2.1 %copy.23 = bf16[192,2048]{1,0:T(8,128)(2,1)} copy(bf16[192,2048]{1,0:T(8,128)(2,1)} %shard_map.109) | data formatting | bytes 1572864
  (8 shorter events, 0.1 us)
Async XLA Ops:
  1.6 0.8 copy-start
  2.6 0.8 copy-start.1
